TPU v7x, 32 devices: a whole 2x2x4 slice. The times are simulated.
32 devices in a mesh: fs: 8 (over z, y), tp: 4 (over x, core).
Axes of the slice: x: 2, y: 2, z: 4, core: 2. Of those that a mesh axis runs over, the one named last changes fastest.
Arguments:
- prompt: bfloat16 [6144, 2048], P('fs'), may hold values from -6 to 6
- routes: int32 [6144, 2], P('fs'), may hold values from 0 to 15, all different within a row; in each aligned block of 768 rows (0 to 767, 768 to 1535, ...) at most 192 rows name the same one
- affinity: float32 [6144, 2], P('fs'), may hold values from 0.05 to 1
- norm_gain: float32 [2048], P('fs'), may hold values from 0.1 to 1.9
- gate_master: float32 [16, 2048, 1024], P(None, 'fs', 'tp'), may hold values from -0.125 to 0.125
- up_master: float32 [16, 2048, 1024], P(None, 'fs', 'tp'), may hold values from -0.125 to 0.125
- down_master: float32 [16, 1024, 2048], P(None, 'fs', 'tp'), may hold values from -0.1875 to 0.1875
Outputs:
- mixed: bfloat16 [6144, 2048], P('fs', 'tp')
- gate_weights: bfloat16 [16, 2048, 1024], P('fs', None, 'tp')
- up_weights: bfloat16 [16, 2048, 1024], P('fs', None, 'tp')
- down_weights: bfloat16 [16, 1024, 2048], P('fs', None, 'tp')
Inputs may be any that keep to these rules, and one draw needn't show every extreme that they name: `routes`: each row names 2 different experts. In each aligned block of 768 rows no expert is named more than 192 times, a bound that some block reaches.
All inputs are finite; a program needn't handle non-finite values.
Results may differ from a plain program's by a relative error of at most 0.0086.
Values may be sent and summed in bfloat16 or wider, within the bound.
A program may use at most 128 MiB of HBM per device.

v0:
```python
import jax
import jax.numpy as jnp
from jax import lax
from jax.sharding import PartitionSpec as P

norm_eps = 1e-06


def per_device(prompt, routes, affinity, norm_gain, gate_master, up_master, down_master):
    tp_count = lax.axis_size("tp")
    experts = gate_master.shape[0]
    gain_rows = norm_gain[None, :, None]
    gate_half = (gate_master * gain_rows).astype(jnp.bfloat16)
    up_half = (up_master * gain_rows).astype(jnp.bfloat16)
    down_half = down_master.astype(jnp.bfloat16)
    gate_new, up_new, down_new = (
        lax.all_to_all(gate_half, "fs", split_axis=0, concat_axis=1, tiled=True),
        lax.all_to_all(up_half, "fs", split_axis=0, concat_axis=1, tiled=True),
        lax.all_to_all(down_half, "fs", split_axis=0, concat_axis=1, tiled=True),
    )
    token_count = prompt.shape[0]
    top_count = routes.shape[1]
    model_width = prompt.shape[1]
    capacity = 2 * token_count * top_count // experts
    flat_ids = routes.reshape(-1)
    onehot = (flat_ids[:, None] == jnp.arange(experts, dtype=jnp.int32)[None, :]).astype(jnp.int32)
    slot_rank = jnp.sum(jnp.cumsum(onehot, axis=0) * onehot, axis=1) - 1
    slot_index = flat_ids * capacity + slot_rank
    values = prompt.astype(jnp.float32)
    normed = (
        values * lax.rsqrt(jnp.mean(values * values, axis=-1, keepdims=True) + norm_eps)
    ).astype(jnp.bfloat16)
    column_width = model_width // tp_count
    column_slice = lax.dynamic_slice_in_dim(
        normed, lax.axis_index("tp") * column_width, column_width, 1
    )
    slot_rows = jnp.broadcast_to(
        column_slice[:, None, :], (token_count, top_count, column_width)
    ).reshape(-1, column_width)
    outbox = (
        jnp.zeros((experts * capacity, column_width), jnp.bfloat16).at[slot_index].set(slot_rows)
    )
    received = lax.all_to_all(
        outbox.reshape(experts, capacity, column_width),
        "fs",
        split_axis=0,
        concat_axis=1,
        tiled=True,
    )
    shard_piece = lax.all_gather(received, "tp", axis=2, tiled=True)
    gate_pre = jnp.einsum("erd,edf->erf", shard_piece, gate_new, preferred_element_type=jnp.float32)
    up_pre = jnp.einsum("erd,edf->erf", shard_piece, up_new, preferred_element_type=jnp.float32)
    hidden = (jax.nn.silu(gate_pre) * up_pre).astype(jnp.bfloat16)
    expert_out = jnp.einsum(
        "erf,efd->erd",
        lax.all_gather(hidden, "tp", axis=2, tiled=True),
        down_new,
        preferred_element_type=jnp.float32,
    ).astype(jnp.bfloat16)
    returned = lax.all_to_all(expert_out, "fs", split_axis=1, concat_axis=0, tiled=True)
    picked = returned.reshape(experts * capacity, -1)[slot_index].reshape(
        token_count, top_count, -1
    )
    share = affinity / jnp.sum(affinity, axis=1, keepdims=True)
    mixed_out = jnp.sum(share[:, :, None] * picked.astype(jnp.float32), axis=1).astype(jnp.bfloat16)
    return (mixed_out, gate_new, up_new, down_new)


def solution(mesh):
    in_specs = (
        P("fs", None),
        P("fs", None),
        P("fs", None),
        P("fs"),
        P(None, "fs", "tp"),
        P(None, "fs", "tp"),
        P(None, "fs", "tp"),
    )
    out_specs = (P("fs", "tp"), P("fs", None, "tp"), P("fs", None, "tp"), P("fs", None, "tp"))
    return jax.shard_map(
        per_device, mesh=mesh, in_specs=in_specs, out_specs=out_specs, check_vma=False
    )
```

profile of v0, /device:TPU:0, one launch (start us, length us, event | category | flops | bytes accessed | tf_op | source)
XLA Modules:
  0.0 415.7 jit_solution(1486511476478039766)
XLA Ops:
  7.2 0.0 all-gather.3.cloned.1.call-start
  7.2 0.7 broadcast_multiply_fusion
  7.9 0.9 copy.27
  8.8 0.2 eq.29
  9.0 0.2 eq.25
  9.2 0.0 copy-start.1
  9.2 5.5 %convert_element_type.36 = f32[768,2048]{1,0:T(8,128)} convert(bf16[768,2048]{1,0:T(8,128)(2,1)} %param.7) | non-fusion elementwise | flops 1572864 | bytes 9437184 | tf_op jit(solution)/shard_map/convert_element_type | solution.py:29
  14.8 0.0 copy-done.1
  14.8 0.7 multiply_reduce_fusion
  15.5 0.2 copy.26
  15.7 0.3 mul.65
  15.9 4.5 %reduce-window.6 = s32[16,12,128]{2,1,0:T(8,128)S(1)} reduce-window(s32[16,12,128]{2,1,0:T(8,128)S(1)} %fusion.4, s32[]{:T(128)} %constant.15.clone.1), window={size=1x1x128 pad=0_0x0_0x127_0}, to_apply=%region_1.2 | reduce-window | flops 3121152 | bytes 196612 | tf_op jit(solution)/shard_map/reduce-window
  20.5 0.4 slice_reduce_fusion
  20.9 0.2 reduce-window.9
  21.1 0.1 broadcast_add_fusion
  21.3 1.6 fusion.1
  22.9 0.8 broadcast_in_dim.5
  23.7 2.0 reshape.101
  25.7 8.8 %scatter_custom_fusion = bf16[3072,512]{1,0:T(8,128)(2,1)S(1)} fusion(s32[1536]{0:T(1024)S(1)} %fusion.7, bf16[1536,512]{1,0:T(8,128)(2,1)} %reshape.101, bf16[]{:T(256)} %constant.13.clone.1), kind=kCustom, calls=%fused_computation.11 | custom fusion | bytes 3146240 | tf_op jit(solution)/shard_map/scatter | solution.py:41
  34.6 77.8 %all_to_all.87 = bf16[16,192,512]{2,1,0:T(8,128)(2,1)S(1)} all-to-all(bf16[16,192,512]{2,1,0:T(8,128)(2,1)S(1)} %bitcast.44), channel_id=1, replica_groups=mesh['fs'=8,'tp'=4] {'fs'}, dimensions={0} | all-to-all | bytes 6291456 | tf_op jit(solution)/shard_map/all_to_all | solution.py:43
  112.4 1.9 copy.29
  114.3 0.0 copy-start.5
  114.4 0.0 all-gather.3.cloned.1.call-update
  114.4 0.7 copy-done.5
  115.0 5.8 %multiply_convert_fusion.1 = (bf16[16,256,256]{2,1,0:T(8,128)(2,1)}, bf16[16,256,256]{2,1,0:T(8,128)(2,1)S(1)}) fusion(f32[16,256,256]{2,1,0:T(8,128)} %param.11, f32[256]{0:T(256)S(1)} %copy-done.5, f32[16,256,256]{2,1,0:T(8,128)} %param.12), kind=kLoop, calls=%fused_computation.4 | loop fusion | flops 4194304 | bytes 12583936 | tf_op jit(solution)/shard_map/convert_element_type | solution.py:13
  120.8 51.5 %all_to_all.88 = bf16[16,256,256]{2,1,0:T(8,128)(2,1)} all-to-all(bf16[16,256,256]{2,1,0:T(8,128)(2,1)S(1)} %get-tuple-element.5), channel_id=1, replica_groups=mesh['fs'=8,'tp'=4] {'fs'}, dimensions={0} | all-to-all | bytes 4194304 | tf_op jit(solution)/shard_map/all_to_all | solution.py:18
  172.3 3.6 all-to-all-start.1
  175.9 0.2 all-gather.5.cloned.1.call-start
  176.2 3.1 copy.31
  179.2 44.4 %all-to-all-done.1 = bf16[16,256,256]{2,1,0:T(8,128)(2,1)S(1)} async-done(((bf16[16,256,256]{2,1,0:T(8,128)(2,1)}), bf16[16,256,256]{2,1,0:T(8,128)(2,1)S(1)}, u32[]{:S(2)}, u32[]{:S(2)}) %all-to-all-start.1) | async-done | bytes 2097184 | tf_op jit(solution)/shard_map/all_to_all | solution.py:17
  223.6 1.5 copy.30
  225.1 0.0 all-gather.3.cloned.1.call-done
  225.1 0.0 copy-start.2
  225.1 0.0 copy-start.6
  225.1 7.2 %fusion.8 = f32[2,1536,256]{2,1,0:T(8,128)S(1)} fusion(bf16[2,1536,2048]{2,1,0:T(8,128)(2,1)} %all-gather.3.cloned.1.call-done, bf16[2,2048,256]{2,1,0:T(8,128)(2,1)} %bitcast.51), kind=kOutput, calls=%fused_computation.28 | convolution fusion | flops 3221225472 | bytes 17825792 | tf_op jit(solution)/shard_map/erd,edf->erf/dot_general | solution.py:51
  232.3 0.0 copy-done.2
  232.3 2.2 copy-done.6
  234.5 5.0 %fusion = bf16[2,1536,256]{2,1,0:T(8,128)(2,1)} fusion(bf16[2,1536,2048]{2,1,0:T(8,128)(2,1)S(1)} %copy-done.6, bf16[2,2048,256]{2,1,0:T(8,128)(2,1)S(1)} %bitcast.50, f32[2,1536,256]{2,1,0:T(8,128)S(1)} %fusion.8), kind=kOutput, calls=%fused_computation.8 | convolution fusion | flops 3225944064 | bytes 19398656 | tf_op jit(solution)/shard_map/erd,edf->erf/dot_general | solution.py:52
  239.6 0.0 all-gather.5.cloned.1.call-update
  239.6 2.5 convert_element_type.41
  242.1 51.8 %all_to_all.89 = bf16[16,128,512]{2,1,0:T(8,128)(2,1)S(1)} all-to-all(bf16[16,128,512]{2,1,0:T(8,128)(2,1)S(1)} %convert_element_type.41), channel_id=1, replica_groups=mesh['fs'=8,'tp'=4] {'fs'}, dimensions={0} | all-to-all | bytes 4194304 | tf_op jit(solution)/shard_map/all_to_all | solution.py:19
  293.9 0.2 copy.32
  294.1 0.0 copy-start.3
  294.1 0.0 all-gather.5.cloned.1.call-done
  294.1 7.3 %convolution_convert_fusion = bf16[2,1536,512]{2,1,0:T(8,128)(2,1)S(1)} fusion(bf16[2,1536,1024]{2,1,0:T(8,128)(2,1)} %all-gather.5.cloned.1.call-done, bf16[2,1024,512]{2,1,0:T(8,128)(2,1)S(1)} %bitcast.53), kind=kOutput, calls=%fused_computation.5 | convolution fusion | flops 3222798336 | bytes 11534336 | tf_op jit(solution)/shard_map/erf,efd->erd/dot_general | solution.py:54
  301.4 0.0 copy-done.3
  301.4 14.5 %copy.33 = bf16[2,1536,512]{2,0,1:T(2,128)(2,1)} copy(bf16[2,1536,512]{2,1,0:T(8,128)(2,1)S(1)} %convolution_convert_fusion) | data formatting | bytes 6291456 | tf_op jit(solution)/shard_map/convert_element_type | solution.py:59
  315.9 0.0 copy-start.4
  315.9 4.0 all-to-all-start.4
  319.9 0.0 copy-done.4
  320.0 0.2 copy.25
  320.2 70.0 %all-to-all-done.4 = bf16[2,1536,512]{2,0,1:T(2,128)(2,1)S(1)} async-done(((bf16[2,1536,512]{2,0,1:T(2,128)(2,1)}), bf16[2,1536,512]{2,0,1:T(2,128)(2,1)S(1)}, u32[]{:S(2)}, u32[]{:S(2)}) %all-to-all-start.4) | async-done | bytes 3145760 | tf_op jit(solution)/shard_map/all_to_all | solution.py:60
  390.2 0.0 copy-start
  390.2 1.7 copy-done
  391.8 2.5 copy.34
  394.3 5.4 %gather_fusion = bf16[1536,512]{1,0:T(8,128)(2,1)} fusion(bf16[3072,512]{1,0:T(8,128)(2,1)S(1)} %bitcast.41, s32[2048]{0:T(1024)S(1)} %pad_clamp_fusion), kind=kCustom, calls=%fused_computation | custom fusion | bytes 3151872 | tf_op jit(solution)/shard_map/gather | solution.py:61
  399.8 3.4 reshape.88
  403.2 5.7 %multiply_reduce_fusion.1 = bf16[768,512]{1,0:T(8,128)(2,1)} fusion(f32[768,2,512]{2,1,0:T(2,128)S(1)} %reshape.88, f32[768,2]{1,0:T(8,128)S(1)} %copy.25), kind=kLoop, calls=%fused_computation.7 | loop fusion | flops 1179648 | bytes 3938304 | tf_op jit(solution)/shard_map/reduce_sum | solution.py:65
  (8 shorter events, 0.1 us)
Async XLA Ops:
  7.2 217.9 %all-gather.3.cloned.1.call-start = ((), (), s32[]{:S(2)}) async-start(), calls=%async_computation.5 | async-start | bytes 15728640 | tf_op jit(solution)/shard_map/all_gather | solution.py:50
  9.2 5.6 %copy-start.1 = (bf16[768,2048]{1,0:T(8,128)(2,1)S(1)}, bf16[768,2048]{1,0:T(8,128)(2,1)}, u32[]{:S(2)}) copy-start(bf16[768,2048]{1,0:T(8,128)(2,1)} %param.7) | copy-start | bytes 9437188
  114.3 0.7 copy-start.5
  172.3 51.3 %all-to-all-start.1 = ((bf16[16,256,256]{2,1,0:T(8,128)(2,1)}), bf16[16,256,256]{2,1,0:T(8,128)(2,1)S(1)}, u32[]{:S(2)}, u32[]{:S(2)}) async-start(bf16[16,256,256]{2,1,0:T(8,128)(2,1)} %get-tuple-element.4), calls=%async_computation.1 | async-start | bytes 4194304 | tf_op jit(solution)/shard_map/all_to_all | solution.py:17
  175.9 118.2 %all-gather.5.cloned.1.call-start = ((), (), s32[]{:S(2)}) async-start(), calls=%async_computation.6 | async-start | bytes 7864320 | tf_op jit(solution)/shard_map/all_gather | solution.py:56
  225.1 7.2 %copy-start.2 = (bf16[8,2,256,256]{3,2,0,1:T(8,128)(2,1)S(1)}, bf16[8,2,256,256]{3,2,0,1:T(8,128)(2,1)}, u32[]{:S(2)}) copy-start(bf16[8,2,256,256]{3,2,0,1:T(8,128)(2,1)} %copy.31) | copy-start | bytes 6291460
  225.1 9.4 %copy-start.6 = (bf16[2,1536,2048]{2,1,0:T(8,128)(2,1)S(1)}, bf16[2,1536,2048]{2,1,0:T(8,128)(2,1)}, u32[]{:S(2)}) copy-start(bf16[2,1536,2048]{2,1,0:T(8,128)(2,1)} %all-gather.3.cloned.1.call-done) | copy-start | bytes 37748740
  294.1 7.4 %copy-start.3 = (bf16[8,2,128,512]{3,2,0,1:T(8,128)(2,1)}, bf16[8,2,128,512]{3,2,0,1:T(8,128)(2,1)S(1)}, u32[]{:S(2)}) copy-start(bf16[8,2,128,512]{3,2,0,1:T(8,128)(2,1)S(1)} %copy.32) | copy-start | bytes 6291460
  315.9 4.0 copy-start.4
  315.9 74.2 %all-to-all-start.4 = ((bf16[2,1536,512]{2,0,1:T(2,128)(2,1)}), bf16[2,1536,512]{2,0,1:T(2,128)(2,1)S(1)}, u32[]{:S(2)}, u32[]{:S(2)}) async-start(bf16[2,1536,512]{2,0,1:T(2,128)(2,1)} %copy.33), calls=%async_computation.4 | async-start | bytes 6291456 | tf_op jit(solution)/shard_map/all_to_all | solution.py:60
  390.2 1.7 copy-start
Sparse Core Ops, SparseCore 0:
  114.5 81.0 all-gather.2
  239.7 46.2 all-gather.4
where the time goes:
time: 417 us; the launch traced here: 416 us
  blocking collectives  181 us (43%)
  waiting for transfers between devices  114 us (27%)
  local copies, waits for them, and re-layouts  51.1 us (12%)
  other arithmetic  27.5 us (7%)
  matrix products  19.5 us (5%)
  between operations  14.3 us (3%)
  starting transfers between devices  7.87 us (2%)
    all_to_all x1, blocking collectives, per_device(): lax.all_to_all(outbox.reshape(experts, capacity, column_width), 'fs', spl...  77.8 us
    all_to_all x1, waiting for transfers between devices, per_device(): lax.all_to_all(expert_out, 'fs', split_axis=1, concat_axis=0, tiled=True)  70 us
    all_to_all x1, blocking collectives, per_device(): lax.all_to_all(down_half, 'fs', split_axis=0, concat_axis=1, tiled=True)  51.8 us
    all_to_all x1, blocking collectives, per_device(): lax.all_to_all(up_half, 'fs', split_axis=0, concat_axis=1, tiled=True)  51.5 us
    all_to_all x1, waiting for transfers between devices, per_device(): lax.all_to_all(gate_half, 'fs', split_axis=0, concat_axis=1, tiled=True)  44.4 us
    convert_element_type x1, local copies, waits for them, and re-layouts, per_device(): expert_out = jnp.einsum('erf,efd->erd', lax.all_gather(hidden, 'tp', axis...  14.5 us
    scatter x1, local copies, waits for them, and re-layouts, per_device(): jnp.zeros((experts * capacity, column_width), jnp.bfloat16).at[slot_index]  8.85 us
  transfers between devices with their start and end apart: 4, of which 2 were waited for; matrix products, arithmetic and copies ran while one was open for 3% of the time, Pallas kernels for 0%

commit v1 on v0

--- a/solution.py
+++ b/solution.py
@@ -57,7 +57,10 @@
         down_new,
         preferred_element_type=jnp.float32,
     ).astype(jnp.bfloat16)
-    returned = lax.all_to_all(expert_out, "fs", split_axis=1, concat_axis=0, tiled=True)
+    size = lax.axis_size("fs")
+    blocks = jnp.stack(jnp.split(expert_out, size, axis=1), axis=0)
+    blocks = lax.all_to_all(blocks, "fs", split_axis=0, concat_axis=0)
+    returned = jnp.concatenate(blocks, axis=0)
     picked = returned.reshape(experts * capacity, -1)[slot_index].reshape(
         token_count, top_count, -1
     )

time: 417 us -> 404 us (0.969)
  local copies, waits for them, and re-layouts: 51.1 us -> 38.7 us
    convert_element_type x1 -> x0, local copies, waits for them, and re-layouts: 14.5 us -> none  [per_device(): expert_out = jnp.einsum('erf,efd->erd', lax.all_gather(hidden, 'tp', axis...]
    unnamed x15 -> x20, local copies, waits for them, and re-layouts: 5.42 us -> 9.19 us
where the time goes in v1:
time: 404 us; the launch traced here: 403 us
  blocking collectives  181 us (45%)
  waiting for transfers between devices  115 us (28%)
  local copies, waits for them, and re-layouts  38.7 us (10%)
  other arithmetic  27.5 us (7%)
  matrix products  19.5 us (5%)
  between operations  14.3 us (4%)
  starting transfers between devices  7.65 us (2%)
    all_to_all x1, blocking collectives, per_device(): lax.all_to_all(outbox.reshape(experts, capacity, column_width), 'fs', spl...  77.8 us
    all_to_all x1, waiting for transfers between devices, per_device(): blocks = lax.all_to_all(blocks, 'fs', split_axis=0, concat_axis=0)  70.1 us
    all_to_all x1, blocking collectives, per_device(): lax.all_to_all(down_half, 'fs', split_axis=0, concat_axis=1, tiled=True)  51.8 us
    all_to_all x1, blocking collectives, per_device(): lax.all_to_all(up_half, 'fs', split_axis=0, concat_axis=1, tiled=True)  51.5 us
    all_to_all x1, waiting for transfers between devices, per_device(): lax.all_to_all(gate_half, 'fs', split_axis=0, concat_axis=1, tiled=True)  44.4 us
    unnamed x20, local copies, waits for them, and re-layouts  9.19 us
    scatter x1, local copies, waits for them, and re-layouts, per_device(): jnp.zeros((experts * capacity, column_width), jnp.bfloat16).at[slot_index]  8.85 us
  transfers between devices with their start and end apart: 4, of which 2 were waited for; matrix products, arithmetic and copies ran while one was open for 3% of the time, Pallas kernels for 0%

profile of v1, /device:TPU:0, one launch (start us, length us, event | category | flops | bytes accessed | tf_op | source)
XLA Modules:
  0.0 403.2 jit_solution(7655566963947066297)
XLA Ops:
  7.2 0.0 all-gather.3.cloned.1.call-start
  7.2 0.7 broadcast_multiply_fusion
  7.9 0.9 copy.17
  8.8 0.2 eq.29
  9.0 0.2 eq.25
  9.2 0.0 copy-start
  9.2 5.5 %convert_element_type.36 = f32[768,2048]{1,0:T(8,128)} convert(bf16[768,2048]{1,0:T(8,128)(2,1)} %param.7) | non-fusion elementwise | flops 1572864 | bytes 9437184 | tf_op jit(solution)/shard_map/convert_element_type | solution.py:29
  14.8 0.0 copy-done
  14.8 0.7 multiply_reduce_fusion
  15.5 0.2 copy.16
  15.7 0.3 mul.65
  15.9 4.5 %reduce-window.6 = s32[16,12,128]{2,1,0:T(8,128)S(1)} reduce-window(s32[16,12,128]{2,1,0:T(8,128)S(1)} %fusion.12, s32[]{:T(128)} %constant.15.clone.1), window={size=1x1x128 pad=0_0x0_0x127_0}, to_apply=%region_1.2 | reduce-window | flops 3121152 | bytes 196612 | tf_op jit(solution)/shard_map/reduce-window
  20.5 0.4 slice_reduce_fusion
  20.9 0.2 reduce-window.9
  21.1 0.1 broadcast_add_fusion
  21.3 1.6 fusion.1
  22.9 0.8 broadcast_in_dim.5
  23.7 2.0 reshape.96
  25.7 8.8 %scatter_custom_fusion = bf16[3072,512]{1,0:T(8,128)(2,1)S(1)} fusion(s32[1536]{0:T(1024)S(1)} %fusion.15, bf16[1536,512]{1,0:T(8,128)(2,1)} %reshape.96, bf16[]{:T(256)} %constant.13.clone.1), kind=kCustom, calls=%fused_computation.11 | custom fusion | bytes 3146240 | tf_op jit(solution)/shard_map/scatter | solution.py:41
  34.6 77.8 %all_to_all.77 = bf16[16,192,512]{2,1,0:T(8,128)(2,1)S(1)} all-to-all(bf16[16,192,512]{2,1,0:T(8,128)(2,1)S(1)} %bitcast.72), channel_id=1, replica_groups=mesh['fs'=8,'tp'=4] {'fs'}, dimensions={0} | all-to-all | bytes 6291456 | tf_op jit(solution)/shard_map/all_to_all | solution.py:43
  112.4 1.9 copy.19
  114.3 0.0 copy-start.4
  114.4 0.0 all-gather.3.cloned.1.call-update
  114.4 0.7 copy-done.4
  115.0 5.8 %multiply_convert_fusion.1 = (bf16[16,256,256]{2,1,0:T(8,128)(2,1)}, bf16[16,256,256]{2,1,0:T(8,128)(2,1)S(1)}) fusion(f32[16,256,256]{2,1,0:T(8,128)} %param.11, f32[256]{0:T(256)S(1)} %copy-done.4, f32[16,256,256]{2,1,0:T(8,128)} %param.12), kind=kLoop, calls=%fused_computation.4 | loop fusion | flops 4194304 | bytes 12583936 | tf_op jit(solution)/shard_map/convert_element_type | solution.py:13
  120.8 51.5 %all_to_all.78 = bf16[16,256,256]{2,1,0:T(8,128)(2,1)} all-to-all(bf16[16,256,256]{2,1,0:T(8,128)(2,1)S(1)} %get-tuple-element.5), channel_id=1, replica_groups=mesh['fs'=8,'tp'=4] {'fs'}, dimensions={0} | all-to-all | bytes 4194304 | tf_op jit(solution)/shard_map/all_to_all | solution.py:18
  172.3 3.6 all-to-all-start.1
  175.9 0.2 all-gather.5.cloned.1.call-start
  176.2 3.1 copy.21
  179.2 44.4 %all-to-all-done.1 = bf16[16,256,256]{2,1,0:T(8,128)(2,1)S(1)} async-done(((bf16[16,256,256]{2,1,0:T(8,128)(2,1)}), bf16[16,256,256]{2,1,0:T(8,128)(2,1)S(1)}, u32[]{:S(2)}, u32[]{:S(2)}) %all-to-all-start.1) | async-done | bytes 2097184 | tf_op jit(solution)/shard_map/all_to_all | solution.py:17
  223.6 1.5 copy.20
  225.1 0.0 all-gather.3.cloned.1.call-done
  225.1 0.0 copy-start.1
  225.1 0.0 copy-start.5
  225.1 7.2 %fusion.16 = f32[2,1536,256]{2,1,0:T(8,128)S(1)} fusion(bf16[2,1536,2048]{2,1,0:T(8,128)(2,1)} %all-gather.3.cloned.1.call-done, bf16[2,2048,256]{2,1,0:T(8,128)(2,1)} %bitcast.79), kind=kOutput, calls=%fused_computation.44 | convolution fusion | flops 3221225472 | bytes 17825792 | tf_op jit(solution)/shard_map/erd,edf->erf/dot_general | solution.py:51
  232.3 0.0 copy-done.1
  232.3 2.2 copy-done.5
  234.5 5.0 %fusion = bf16[2,1536,256]{2,1,0:T(8,128)(2,1)} fusion(bf16[2,1536,2048]{2,1,0:T(8,128)(2,1)S(1)} %copy-done.5, bf16[2,2048,256]{2,1,0:T(8,128)(2,1)S(1)} %bitcast.78, f32[2,1536,256]{2,1,0:T(8,128)S(1)} %fusion.16), kind=kOutput, calls=%fused_computation.8 | convolution fusion | flops 3225944064 | bytes 19398656 | tf_op jit(solution)/shard_map/erd,edf->erf/dot_general | solution.py:52
  239.6 0.0 all-gather.5.cloned.1.call-update
  239.6 2.5 convert_element_type.41
  242.1 51.8 %all_to_all.79 = bf16[16,128,512]{2,1,0:T(8,128)(2,1)S(1)} all-to-all(bf16[16,128,512]{2,1,0:T(8,128)(2,1)S(1)} %convert_element_type.41), channel_id=1, replica_groups=mesh['fs'=8,'tp'=4] {'fs'}, dimensions={0} | all-to-all | bytes 4194304 | tf_op jit(solution)/shard_map/all_to_all | solution.py:19
  293.9 0.2 copy.22
  294.1 0.0 copy-start.2
  294.1 0.0 all-gather.5.cloned.1.call-done
  294.1 7.3 %convolution_convert_fusion = bf16[2,1536,512]{2,1,0:T(8,128)(2,1)S(1)} fusion(bf16[2,1536,1024]{2,1,0:T(8,128)(2,1)} %all-gather.5.cloned.1.call-done, bf16[2,1024,512]{2,1,0:T(8,128)(2,1)S(1)} %bitcast.81), kind=kOutput, calls=%fused_computation.5 | convolution fusion | flops 3222798336 | bytes 11534336 | tf_op jit(solution)/shard_map/erf,efd->erd/dot_general | solution.py:54
  301.4 0.0 copy-done.2
  301.4 0.8 fusion.11
  302.2 0.8 fusion.10
  303.0 0.8 fusion.9
  303.7 0.8 fusion.8
  304.5 0.8 fusion.7
  305.3 0.8 fusion.6
  306.1 0.8 fusion.5
  306.9 0.8 fusion.4
  307.7 0.0 copy-start.3
  307.7 3.8 all-to-all-start.4
  311.4 0.0 copy-done.3
  311.5 0.2 copy.15
  311.7 70.1 %all-to-all-done.4 = bf16[8,2,192,512]{3,2,1,0:T(8,128)(2,1)S(1)} async-done(((bf16[8,2,192,512]{3,2,1,0:T(8,128)(2,1)}), bf16[8,2,192,512]{3,2,1,0:T(8,128)(2,1)S(1)}, u32[]{:S(2)}, u32[]{:S(2)}) %all-to-all-start.4) | async-done | bytes 3145760 | tf_op jit(solution)/shard_map/all_to_all | solution.py:62
  381.8 5.4 %gather_fusion = bf16[1536,512]{1,0:T(8,128)(2,1)} fusion(bf16[3072,512]{1,0:T(8,128)(2,1)S(1)} %bitcast.70, s32[2048]{0:T(1024)S(1)} %pad_clamp_fusion), kind=kCustom, calls=%fused_computation | custom fusion | bytes 3151872 | tf_op jit(solution)/shard_map/gather | solution.py:64
  387.2 3.4 reshape.83
  390.6 5.7 %multiply_reduce_fusion.1 = bf16[768,512]{1,0:T(8,128)(2,1)} fusion(f32[768,2,512]{2,1,0:T(2,128)S(1)} %reshape.83, f32[768,2]{1,0:T(8,128)S(1)} %copy.15), kind=kLoop, calls=%fused_computation.7 | loop fusion | flops 1179648 | bytes 3938304 | tf_op jit(solution)/shard_map/reduce_sum | solution.py:68
  (8 shorter events, 0.1 us)
Async XLA Ops:
  7.2 217.9 %all-gather.3.cloned.1.call-start = ((), (), s32[]{:S(2)}) async-start(), calls=%async_computation.5 | async-start | bytes 15728640 | tf_op jit(solution)/shard_map/all_gather | solution.py:50
  9.2 5.6 %copy-start = (bf16[768,2048]{1,0:T(8,128)(2,1)S(1)}, bf16[768,2048]{1,0:T(8,128)(2,1)}, u32[]{:S(2)}) copy-start(bf16[768,2048]{1,0:T(8,128)(2,1)} %param.7) | copy-start | bytes 9437188
  114.3 0.7 copy-start.4
  172.3 51.3 %all-to-all-start.1 = ((bf16[16,256,256]{2,1,0:T(8,128)(2,1)}), bf16[16,256,256]{2,1,0:T(8,128)(2,1)S(1)}, u32[]{:S(2)}, u32[]{:S(2)}) async-start(bf16[16,256,256]{2,1,0:T(8,128)(2,1)} %get-tuple-element.4), calls=%async_computation.1 | async-start | bytes 4194304 | tf_op jit(solution)/shard_map/all_to_all | solution.py:17
  175.9 118.2 %all-gather.5.cloned.1.call-start = ((), (), s32[]{:S(2)}) async-start(), calls=%async_computation.6 | async-start | bytes 7864320 | tf_op jit(solution)/shard_map/all_gather | solution.py:56
  225.1 7.2 %copy-start.1 = (bf16[8,2,256,256]{3,2,0,1:T(8,128)(2,1)S(1)}, bf16[8,2,256,256]{3,2,0,1:T(8,128)(2,1)}, u32[]{:S(2)}) copy-start(bf16[8,2,256,256]{3,2,0,1:T(8,128)(2,1)} %copy.21) | copy-start | bytes 6291460
  225.1 9.4 %copy-start.5 = (bf16[2,1536,2048]{2,1,0:T(8,128)(2,1)S(1)}, bf16[2,1536,2048]{2,1,0:T(8,128)(2,1)}, u32[]{:S(2)}) copy-start(bf16[2,1536,2048]{2,1,0:T(8,128)(2,1)} %all-gather.3.cloned.1.call-done) | copy-start | bytes 37748740
  294.1 7.4 %copy-start.2 = (bf16[8,2,128,512]{3,2,0,1:T(8,128)(2,1)}, bf16[8,2,128,512]{3,2,0,1:T(8,128)(2,1)S(1)}, u32[]{:S(2)}) copy-start(bf16[8,2,128,512]{3,2,0,1:T(8,128)(2,1)S(1)} %copy.22) | copy-start | bytes 6291460
  307.7 3.8 copy-start.3
  307.7 74.1 %all-to-all-start.4 = ((bf16[8,2,192,512]{3,2,1,0:T(8,128)(2,1)}), bf16[8,2,192,512]{3,2,1,0:T(8,128)(2,1)S(1)}, u32[]{:S(2)}, u32[]{:S(2)}) async-start(bf16[8,2,192,512]{3,2,1,0:T(8,128)(2,1)} %fusion.4), calls=%async_computation.4 | async-start | bytes 6291456 | tf_op jit(solution)/shard_map/all_to_all | solution.py:62
Sparse Core Ops, SparseCore 0:
  114.5 81.0 all-gather.2
  239.7 46.2 all-gather.4
